TPU v7x, 32 devices: a whole 2x2x4 slice. The times are simulated.
32 devices in a mesh: sp: 4 (over z), fs: 4 (over y, core), tp: 2 (over x).
Axes of the slice: x: 2, y: 2, z: 4, core: 2. Of those that a mesh axis runs over, the one named last changes fastest.
Arguments:
- tokens: bfloat16 [4, 768, 2048], P('fs', 'sp'), may hold values from -6 to 6
- decay_pace: float32 [4, 768], P('fs', 'sp'), may hold values from 0.5 to 2, as said below
- start_state: float32 [4, 16, 64, 64], P('fs', 'tp'), may hold values from -80 to 80
- norm_gain: float32 [2048], replicated, may hold values from 0.1 to 1.9
- conv_value: bfloat16 [2048, 512], P(('sp', 'fs'), 'tp'), may hold values from -0.125 to 0.125
- conv_admit: bfloat16 [2048, 512], P(('sp', 'fs'), 'tp'), may hold values from -0.125 to 0.125
- conv_gate: bfloat16 [2048, 512], P(('sp', 'fs'), 'tp'), may hold values from -0.125 to 0.125
- state_query: bfloat16 [2048, 1024], P(('sp', 'fs'), 'tp'), may hold values from -0.125 to 0.125
- state_key: bfloat16 [2048, 1024], P(('sp', 'fs'), 'tp'), may hold values from -0.125 to 0.125
- state_value: bfloat16 [2048, 1024], P(('sp', 'fs'), 'tp'), may hold values from -0.125 to 0.125
- state_decay: bfloat16 [2048, 1024], P(('sp', 'fs'), 'tp'), may hold values from -0.125 to 0.125
- state_gate: bfloat16 [2048, 1024], P(('sp', 'fs'), 'tp'), may hold values from -0.125 to 0.125
- conv_taps: float32 [31, 512], P(None, 'tp'), may hold values from -4 to 4
- conv_gain: float32 [512], P('tp'), may hold values from 0.1 to 1.9
- point_weight: bfloat16 [512, 512], replicated, may hold values from -0.25 to 0.25
- decay_base: float32 [1024], P('tp'), may hold values from -13 to -3
- correction: float32 [1024], P('tp'), may hold values from 0 to 0.9
- group_gain: float32 [1024], P('tp'), may hold values from 0.1 to 1.9
- output_conv: bfloat16 [512, 2048], P('tp', ('sp', 'fs')), may hold values from -0.25 to 0.25
- output_state: bfloat16 [1024, 2048], P('tp', ('sp', 'fs')), may hold values from -0.1875 to 0.1875
Outputs:
- mixed: bfloat16 [4, 768, 2048], P('fs', ('sp', 'tp'))
Inputs may be any that keep to these rules, and one draw needn't show every extreme that they name: `decay_pace`: constant over runs of positions, a quarter of 192 long.
All inputs are finite; a program needn't handle non-finite values.
Results may differ from a plain program's by a relative error of at most 0.017.
Values may be sent and summed in bfloat16 or wider, within the bound.
A program may use at most 64 MiB of HBM per device.

v0:
```python
import jax
import jax.numpy as jnp
from jax import lax
from jax.sharding import PartitionSpec as P

NORM_FLOOR = 0.1
CHANNEL_FLOOR = 0.1
GROUP_FLOOR = 1.0


def passed_along(value, axis, steps):
    count = lax.axis_size(axis)
    leading, last = (max(0, -steps), min(count, count - steps))
    return lax.ppermute(value, axis, [(source, source + steps) for source in range(leading, last)])


def entering_2(value, axis, join, neutral):
    place = lax.axis_index(axis)
    gathered = jax.tree.map(
        lambda a, kind: lax.all_gather(a.astype(kind), axis),
        value,
        jax.tree.map(lambda a: jnp.bfloat16 if a.dtype == jnp.float32 else a.dtype, value),
    )
    state = jax.tree.map(lambda a, e: jnp.zeros_like(a) + jnp.asarray(e, a.dtype), value, neutral)

    def one(lap, state):
        return join(
            state,
            jax.tree.map(
                lambda a, own: lax.dynamic_index_in_dim(a, lap, 0, False).astype(own.dtype),
                gathered,
                value,
            ),
        )

    return lax.fori_loop(0, place, one, state)


def apply_map(matrix, right):
    return jnp.einsum("hbti,hbic->hbtc", matrix, right, precision=lax.Precision.HIGHEST)


def pair_terms(left, right, mask):
    return jnp.einsum("hbtc,hbic->hbti", left, right, precision=lax.Precision.HIGHEST) * mask


def compose(earlier, later):
    first = jnp.matmul(earlier[0], later[0], precision=lax.Precision.HIGHEST)
    second = jnp.matmul(earlier[1], later[0], precision=lax.Precision.HIGHEST) + later[1]
    return (first, second)


def block_terms(query, keys, values, unit, write, log_keep):
    size = query.shape[-1]
    span = query.shape[2]
    total_log = jnp.cumsum(log_keep, axis=2)
    before_log = total_log - log_keep
    last_log = total_log[:, :, span - 1 :, :]
    lead_remove = -unit * jnp.exp(before_log)
    lead_query = query * jnp.exp(total_log)
    back_write = write * jnp.exp(-total_log)
    back_key = keys * jnp.exp(-total_log)
    places = jnp.arange(span)
    strict = (places[:, None] > places[None, :]).astype(jnp.float32)
    weak = (places[:, None] >= places[None, :]).astype(jnp.float32)
    remove_write = pair_terms(lead_remove, back_write, strict)
    remove_key = pair_terms(lead_remove, back_key, strict)
    query_write = pair_terms(lead_query, back_write, weak)
    query_key = pair_terms(lead_query, back_key, weak)
    right_side = jnp.concatenate([apply_map(remove_key, values), lead_remove], axis=-1)
    system = jnp.eye(span, dtype=jnp.float32) - remove_write
    solved = jax.scipy.linalg.solve_triangular(system, right_side, lower=True, unit_diagonal=True)
    own_part = solved[..., :size]
    start_part = solved[..., size:]
    local_out = apply_map(query_write, own_part) + apply_map(query_key, values)
    start_map = lead_query + apply_map(query_write, start_part)
    tail_write = write * jnp.exp(last_log - total_log)
    tail_key = keys * jnp.exp(last_log - total_log)
    carry_map = jnp.einsum(
        "hbtk,hbtj->hbkj", start_part, tail_write, precision=lax.Precision.HIGHEST
    ) + jnp.eye(size, dtype=jnp.float32) * jnp.exp(last_log)
    carry_add = jnp.einsum(
        "hbtv,hbtj->hbvj", own_part, tail_write, precision=lax.Precision.HIGHEST
    ) + jnp.einsum("hbtv,hbtj->hbvj", values, tail_key, precision=lax.Precision.HIGHEST)
    return (local_out, start_map, carry_map, carry_add)


def body(
    tokens,
    decay_pace,
    start_state,
    norm_gain,
    conv_value,
    conv_admit,
    conv_gate,
    state_query,
    state_key,
    state_value,
    state_decay,
    state_gate,
    conv_taps,
    conv_gain,
    point_weight,
    decay_base,
    correction,
    group_gain,
    output_conv,
    output_state,
):
    width = tokens.shape[-1]
    rows = tokens.reshape(-1, width)
    length = rows.shape[0]
    floats = rows.astype(jnp.float32)
    inverse = lax.rsqrt(jnp.mean(floats * floats, axis=1, keepdims=True) + NORM_FLOOR)
    normed = (floats * inverse * norm_gain).astype(jnp.bfloat16)
    shards = (
        conv_value,
        conv_admit,
        conv_gate,
        state_query,
        state_key,
        state_value,
        state_decay,
        state_gate,
    )
    stacked = jnp.concatenate(shards, axis=1)
    projected = jnp.dot(
        normed,
        lax.all_gather(stacked, ("sp", "fs"), axis=0, tiled=True),
        preferred_element_type=jnp.float32,
    ).astype(jnp.bfloat16)
    pieces = []
    offset = 0
    for shard in shards:
        pieces.append(projected[:, offset : offset + shard.shape[1]].astype(jnp.float32))
        offset = offset + shard.shape[1]
    value, admit, gate_conv, query, keys, values, decay_in, gate_state = pieces
    channels = value.shape[1]
    kernel = conv_taps.shape[0]
    conv_input = (value * jax.nn.sigmoid(admit)).astype(jnp.bfloat16)
    earlier = passed_along(conv_input[length - (kernel - 1) :], "sp", 1)
    padded = jnp.concatenate([earlier, conv_input], axis=0).astype(jnp.float32)
    conv_sum = jnp.zeros((length, channels), jnp.float32)
    for place in range(kernel):
        conv_sum = conv_sum + conv_taps[place] * padded[place : place + length]
    local_point = lax.dynamic_slice_in_dim(
        point_weight, lax.axis_index("tp") * channels, channels, 1
    )
    whole_sum, whole_gain = (
        lax.all_gather(conv_sum.astype(jnp.bfloat16), "tp", axis=1, tiled=True).astype(
            conv_sum.dtype
        ),
        lax.all_gather(conv_gain.astype(jnp.bfloat16), "tp", axis=0, tiled=True).astype(
            conv_gain.dtype
        ),
    )
    mean = jnp.mean(whole_sum, axis=1, keepdims=True)
    spread = jnp.mean(whole_sum * whole_sum, axis=1, keepdims=True) - mean * mean
    shaped = jax.nn.silu(
        (whole_sum - mean) * lax.rsqrt(spread + CHANNEL_FLOOR) * whole_gain
    ).astype(jnp.bfloat16)
    pointwise = jnp.dot(shaped, local_point, preferred_element_type=jnp.float32)
    conv_out = (pointwise * jax.nn.silu(gate_conv)).astype(jnp.bfloat16)
    size = start_state.shape[-1]
    heads = query.shape[1] // size
    span = min(64, length)
    blocks = length // span
    log_keep = -jnp.exp(decay_base + jnp.tanh(decay_in)) * decay_pace.reshape(-1)[:, None]
    key_heads = keys.reshape(length, heads, size)
    unit = key_heads * lax.rsqrt(
        jnp.maximum(jnp.sum(key_heads * key_heads, axis=-1, keepdims=True), 1.0)
    )
    write = unit * correction.reshape(heads, size)

    def arrange(array):
        return array.reshape(blocks, span, heads, size).transpose(2, 0, 1, 3)

    local_out, start_map, carry_map, carry_add = block_terms(
        arrange(query),
        arrange(keys),
        arrange(values),
        arrange(unit),
        arrange(write),
        arrange(log_keep),
    )
    identity = (
        jnp.broadcast_to(jnp.eye(size, dtype=jnp.float32), (heads, size, size)),
        jnp.zeros((heads, size, size), jnp.float32),
    )

    def along(carried, block_pair):
        return (compose(carried, block_pair), carried)

    device_pair, prefixes = lax.scan(
        along, identity, (jnp.moveaxis(carry_map, 1, 0), jnp.moveaxis(carry_add, 1, 0))
    )
    prior_map, prior_add = entering_2(device_pair, "sp", compose, identity)
    begin = start_state.reshape(heads, size, size)
    entering = jnp.matmul(begin, prior_map, precision=lax.Precision.HIGHEST) + prior_add
    block_starts = (
        jnp.matmul(entering[None], prefixes[0], precision=lax.Precision.HIGHEST) + prefixes[1]
    )
    block_starts = jnp.moveaxis(block_starts, 0, 1)
    outputs = local_out + jnp.einsum(
        "hbtk,hbvk->hbtv", start_map, block_starts, precision=lax.Precision.HIGHEST
    )
    outputs = outputs.transpose(1, 2, 0, 3).reshape(length, heads, size)
    centered = outputs - jnp.mean(outputs, axis=-1, keepdims=True)
    variance = jnp.mean(centered * centered, axis=-1, keepdims=True)
    grouped = centered * lax.rsqrt(variance + GROUP_FLOOR) * group_gain.reshape(heads, size)
    state_out = (grouped.reshape(length, heads * size) * jax.nn.silu(gate_state)).astype(
        jnp.bfloat16
    )
    local_mix = jnp.concatenate([conv_out, state_out], axis=1)
    moved = lax.all_to_all(local_mix, "tp", split_axis=0, concat_axis=1, tiled=True)
    conv_rows, state_rows = (
        lax.all_gather(output_conv, "tp", axis=0, tiled=True),
        lax.all_gather(output_state, "tp", axis=0, tiled=True),
    )
    groups = lax.axis_size("tp")
    joined = jnp.concatenate(
        [conv_rows.reshape(groups, channels, -1), state_rows.reshape(groups, heads * size, -1)],
        axis=1,
    )
    joined = joined.reshape(groups * (channels + heads * size), -1)
    mixed = jnp.dot(
        moved,
        lax.all_gather(joined, ("sp", "fs"), axis=1, tiled=True),
        preferred_element_type=jnp.float32,
    )
    return mixed.astype(jnp.bfloat16).reshape(1, -1, width)


def solution(mesh):
    return jax.shard_map(
        body,
        mesh=mesh,
        in_specs=(
            P("fs", "sp", None),
            P("fs", "sp"),
            P("fs", "tp", None, None),
            P(),
            P(("sp", "fs"), "tp"),
            P(("sp", "fs"), "tp"),
            P(("sp", "fs"), "tp"),
            P(("sp", "fs"), "tp"),
            P(("sp", "fs"), "tp"),
            P(("sp", "fs"), "tp"),
            P(("sp", "fs"), "tp"),
            P(("sp", "fs"), "tp"),
            P(None, "tp"),
            P("tp"),
            P(),
            P("tp"),
            P("tp"),
            P("tp"),
            P("tp", ("sp", "fs")),
            P("tp", ("sp", "fs")),
        ),
        out_specs=P("fs", ("sp", "tp"), None),
        check_vma=False,
    )
```

profile of v0, /device:TPU:0, one launch (start us, length us, event | category | flops | bytes accessed | tf_op | source)
XLA Modules:
  0.0 373.3 jit_solution(13243552099346474829)
XLA Ops:
  14.9 5.9 %all_gather.37 = bf16[512,128]{1,0:T(8,128)(2,1)S(1)} all-gather(bf16[256,128]{1,0:T(8,128)(2,1)S(1)} %copy-done.24), channel_id=1, replica_groups=mesh['sp'=4,'fs'=4,'tp'=2] {'tp'}, dimensions={0}, use_global_device_ids=true | all-gather | bytes 196608 | tf_op jit(solution)/shard_map/all_gather | solution.py:217
  20.7 5.6 %all_gather.38 = bf16[1024,128]{1,0:T(8,128)(2,1)S(1)} all-gather(bf16[512,128]{1,0:T(8,128)(2,1)S(1)} %copy-done.20), channel_id=1, replica_groups=mesh['sp'=4,'fs'=4,'tp'=2] {'tp'}, dimensions={0}, use_global_device_ids=true | all-gather | bytes 393216 | tf_op jit(solution)/shard_map/all_gather | solution.py:218
  29.5 4.2 %all-gather.2 = bf16[2,1,256]{2,1,0:T(2,128)(2,1)S(1)} all-gather(bf16[1,1,256]{2,1,0:T(2,128)(2,1)S(1)} %reshape.181), channel_id=1, replica_groups=mesh['sp'=4,'fs'=4,'tp'=2] {'tp'}, dimensions={0}, use_global_device_ids=true | all-gather | bytes 1536 | tf_op jit(solution)/shard_map/all_gather | solution.py:153
  35.2 89.4 %all-gather.6.cloned.1.call-done = bf16[2048,3328]{1,0:T(8,128)(2,1)} async-done(((bf16[128,3328]{1,0:T(8,128)(2,1)}), bf16[2048,3328]{1,0:T(8,128)(2,1)}) %all-gather.6.cloned.1.call-update) | async-done | bytes 13631504 | tf_op jit(solution)/shard_map/all_gather | solution.py:129
  124.5 7.8 %convolution_convert_fusion = bf16[192,3328]{1,0:T(8,128)(2,1)S(1)} fusion(bf16[2048,3328]{1,0:T(8,128)(2,1)} %all-gather.6.cloned.1.call-done, bf16[1,192,2048]{2,1,0:T(8,128)(2,1)S(1)} %copy-done.9, f32[2048]{0:T(1024)S(1)} %copy-done.62, f32[192]{0:T(256)S(1)} %add_rsqrt_fusion.2), kind=kOutput, calls=%fused_computation.27 | convolution fusion | flops 2619457536 | bytes 15704832 | tf_op jit(solution)/shard_map/dot_general | solution.py:127
  133.9 2.8 collective-permute-start
  139.0 1.6 bitcast_multiply_fusion.3
  140.6 2.5 convolution_multiply_fusion.1
  143.2 2.6 fusion.30
  145.7 119.3 %custom-call.4 = f32[8,3,1,64,64]{3,4,2,1,0:T(8,128)} custom-call(f32[8,3,1,64,64]{4,3,2,1,0:T(8,128)} %fusion.30), custom_call_target="InvertDiagBlocksLowerTriangular" | custom-call | tf_op jit(solution)/shard_map/jit(_solve_triangular)/vmap(vmap())/triangular_solve | solution.py:72
  267.8 1.7 fusion.68
  269.5 1.6 fusion.35
  271.2 1.7 fusion.49
  272.9 2.8 fusion.22
  275.8 1.7 fusion.26
  277.5 17.8 %while.30 = (s32[]{:T(128)}, f32[8,64,64]{1,2,0:T(8,128)S(1)}, f32[8,64,64]{1,2,0:T(8,128)S(1)}, f32[3,8,64,64]{2,3,1,0:T(8,128)}, f32[3,8,64,64]{3,2,1,0:T(8,12...) while((s32[]{:T(128)}, f32[8,64,64]{1,2,0:T(8,128)S(1)}, ...), condition=%wide.region_6.7_spmd.clone, body=%wide.region_5.6_spmd.clone.sunk | while | flops 50429952 | bytes 3541100 | solution.py:194
  278.7 1.6 fusion.164
  281.9 1.5 convolution_bitcast_fusion.10
  284.7 1.6 fusion.164
  287.8 1.5 convolution_bitcast_fusion.10
  290.6 1.6 fusion.164
  293.8 1.5 convolution_bitcast_fusion.10
  295.6 2.1 reshape.178
  297.7 16.0 %all-gather = bf16[32,64,64]{2,1,0:T(8,128)(2,1)S(1)} all-gather(bf16[8,64,64]{2,1,0:T(8,128)(2,1)S(1)} %copy.105), channel_id=2, replica_groups=mesh['sp'=4,'fs'=4,'tp'=2] {'sp'}, dimensions={0}, use_global_device_ids=true | all-gather | bytes 327680 | tf_op jit(solution)/shard_map/all_gather | solution.py:20
  313.7 15.8 %all-gather.1 = bf16[32,64,64]{2,1,0:T(8,128)(2,1)} all-gather(bf16[8,64,64]{2,1,0:T(8,128)(2,1)S(1)} %copy.106), channel_id=3, replica_groups=mesh['sp'=4,'fs'=4,'tp'=2] {'sp'}, dimensions={0}, use_global_device_ids=true | all-gather | bytes 327680 | tf_op jit(solution)/shard_map/all_gather | solution.py:20
  329.8 1.6 fusion.32
  331.4 1.9 convolution_multiply_fusion.3
  334.9 1.9 fusion.24
  336.8 1.8 convolution_multiply_fusion
  346.5 5.3 %all_gather.31 = bf16[192,512]{1,0:T(8,128)(2,1)S(1)} all-gather(bf16[192,256]{1,0:T(8,128)(2,1)S(1)} %fusion.82), channel_id=1, replica_groups=mesh['sp'=4,'fs'=4,'tp'=2] {'tp'}, dimensions={1}, use_global_device_ids=true | all-gather | bytes 294912 | tf_op jit(solution)/shard_map/all_gather | solution.py:150
  353.3 8.5 %all_to_all.19 = bf16[2,96,768]{2,1,0:T(8,128)(2,1)S(1)} all-to-all(bf16[2,96,768]{2,1,0:T(8,128)(2,1)S(1)} %bitcast.225), channel_id=1, replica_groups=mesh['sp'=4,'fs'=4,'tp'=2] {'tp'}, dimensions={0} | all-to-all | bytes 589824 | tf_op jit(solution)/shard_map/all_to_all | solution.py:215
  361.8 4.7 %fusion.18 = bf16[1,96,2048]{2,1,0:T(8,128)(2,1)} fusion(bf16[96,1536]{1,0:T(8,128)(2,1)S(1)} %bitcast.227, bf16[1536,2048]{1,0:T(8,128)(2,1)} %all-gather.8.cloned.1.call-done), kind=kOutput, calls=%fused_computation.29 | convolution fusion | flops 604176384 | bytes 6979584 | tf_op jit(solution)/shard_map/dot_general | solution.py:226
  (227 shorter events, 38.3 us)
Async XLA Ops:
  6.5 345.5 %copy-start = (bf16[512,512]{1,0:T(8,128)(2,1)S(1)}, bf16[512,512]{1,0:T(8,128)(2,1)}, u32[]{:S(2)}) copy-start(bf16[512,512]{1,0:T(8,128)(2,1)} %param.38) | copy-start | bytes 1572868
  6.5 8.3 %copy-start.24 = (bf16[256,128]{1,0:T(8,128)(2,1)S(1)}, bf16[256,128]{1,0:T(8,128)(2,1)}, u32[]{:S(2)}) copy-start(bf16[256,128]{1,0:T(8,128)(2,1)} %param.42) | copy-start | bytes 196612
  6.5 14.2 %copy-start.20 = (bf16[512,128]{1,0:T(8,128)(2,1)S(1)}, bf16[512,128]{1,0:T(8,128)(2,1)}, u32[]{:S(2)}) copy-start(bf16[512,128]{1,0:T(8,128)(2,1)} %param.43) | copy-start | bytes 393220
  6.5 118.0 %all-gather.6.cloned.1.call-start = ((), (), s32[]{:S(2)}) async-start(), calls=%async_computation.1 | async-start | bytes 14483456 | tf_op jit(solution)/shard_map/all_gather | solution.py:129
  11.9 15.3 %copy-start.25 = (f32[31,256]{1,0:T(8,128)S(1)}, f32[31,256]{1,0:T(8,128)}, u32[]{:S(2)}) copy-start(f32[31,256]{1,0:T(8,128)} %param.36) | copy-start | bytes 95236
  12.8 16.3 %copy-start.9 = (bf16[1,192,2048]{2,1,0:T(8,128)(2,1)S(1)}, bf16[1,192,2048]{2,1,0:T(8,128)(2,1)}, u32[]{:S(2)}) copy-start(bf16[1,192,2048]{2,1,0:T(8,128)(2,1)} %param.24) | copy-start | bytes 2359300
  14.8 14.7 %copy-start.63 = (f32[256]{0:T(256)S(1)}, f32[256]{0:T(256)}, u32[]{:S(2)}) copy-start(f32[256]{0:T(256)} %param.37) | copy-start | bytes 3076
  14.8 19.6 %copy-start.59 = (f32[512]{0:T(512)S(1)}, f32[512]{0:T(512)}, u32[]{:S(2)}) copy-start(f32[512]{0:T(512)} %param.40) | copy-start | bytes 6148
  14.8 109.7 %copy-start.62 = (f32[2048]{0:T(1024)S(1)}, f32[2048]{0:T(1024)}, u32[]{:S(2)}) copy-start(f32[2048]{0:T(1024)} %param.27) | copy-start | bytes 24580
  14.8 347.0 %all-gather.8.cloned.1.call-start = ((), (), s32[]{:S(2)}) async-start(), calls=%async_computation.2 | async-start | bytes 6684672 | tf_op jit(solution)/shard_map/all_gather | solution.py:228
  34.4 108.8 %copy-start.13 = (f32[64,64]{1,0:T(8,128)}, f32[64,64]{1,0:T(8,128)S(1)}, u32[]{:S(2)}) copy-start(f32[64,64]{1,0:T(8,128)S(1)} %get-tuple-element.207) | copy-start | bytes 49156
  34.5 108.7 %copy-start.21 = (f32[8,64]{1,0:T(8,128)}, f32[8,64]{1,0:T(8,128)S(1)}, u32[]{:S(2)}) copy-start(f32[8,64]{1,0:T(8,128)S(1)} %mul.623) | copy-start | bytes 6148
  132.3 4.5 %copy-start.7 = (bf16[192,3328]{1,0:T(8,128)(2,1)}, bf16[192,3328]{1,0:T(8,128)(2,1)S(1)}, u32[]{:S(2)}) copy-start(bf16[192,3328]{1,0:T(8,128)(2,1)S(1)} %convolution_convert_fusion) | copy-start | bytes 3833860
  132.3 4.3 %copy-start.57 = (f32[512]{0:T(512)S(1)}, f32[512]{0:T(512)}, u32[]{:S(2)}) copy-start(f32[512]{0:T(512)} %param.39) | copy-start | bytes 6148
  132.4 4.3 %copy-start.61 = (f32[1,192]{1,0:T(1,128)S(1)}, f32[1,192]{1,0:T(1,128)}, u32[]{:S(2)}) copy-start(f32[1,192]{1,0:T(1,128)} %param.25) | copy-start | bytes 2308
  132.4 4.6 %copy-start.15 = (bf16[192,256]{1,0:T(8,128)(2,1)}, bf16[192,256]{1,0:T(8,128)(2,1)S(1)}, u32[]{:S(2)}) copy-start(bf16[192,256]{1,0:T(8,128)(2,1)S(1)} %multiply_convert_fusion) | copy-start | bytes 294916
  133.9 211.0 %collective-permute-start = (bf16[30,256]{1,0:T(8,128)(2,1)}, bf16[30,256]{1,0:T(8,128)(2,1)}, u32[]{:S(2)}, u32[]{:S(2)}) collective-permute-start(bf16[30,256]{1,0:T(8,128)(2,1)} %slice.304), channel_id=1, source_target_pairs={{0,8},{8,16},{16,24},{1,9},{9,17},{17,25},{2,10},{10,18},{18,26},{... | collective-permute-start | bytes 46088 | tf_op jit(solution)/shard_map/ppermute | solution.py:14
  266.3 9.5 %copy-start.5 = (bf16[3,64,8,64]{3,2,1,0:T(8,128)(2,1)}, bf16[3,64,8,64]{3,2,1,0:T(8,128)(2,1)S(1)}, u32[]{:S(2)}) copy-start(bf16[3,64,8,64]{3,2,1,0:T(8,128)(2,1)S(1)} %reshape.169) | copy-start | bytes 589828
  266.3 3.2 copy-start.12
  295.4 34.1 %copy-start.19 = (f32[64,64]{0,1:T(8,128)S(1)}, f32[64,64]{0,1:T(8,128)}, u32[]{:S(2)}) copy-start(f32[64,64]{0,1:T(8,128)} %copy.96) | copy-start | bytes 49156
  343.3 2.4 copy-start.26
  343.3 2.4 copy-start.27
  343.3 2.4 copy-start.28
  343.3 2.4 copy-start.29
  343.4 2.4 copy-start.30
  343.4 2.4 copy-start.31
  343.4 2.4 copy-start.32
  343.4 2.4 copy-start.33
  343.4 2.4 copy-start.34
  343.4 2.4 copy-start.35
  343.4 2.4 copy-start.36
  346.0 6.0 %copy-start.60 = (f32[2,1,256]{2,1,0:T(1,128)S(1)}, f32[2,1,256]{2,1,0:T(1,128)}, u32[]{:S(2)}) copy-start(f32[2,1,256]{2,1,0:T(1,128)} %convert_element_type.135) | copy-start | bytes 6148
  (35 other events, 70.8 us)
Sparse Core Ops, SparseCore 0:
  14.9 109.5 all-gather.5
  126.7 65.0 all-gather.7
where the time goes:
time: 377 us; the launch traced here: 373 us
  other arithmetic  128 us (34%)
  waiting for transfers between devices  89.4 us (24%)
  blocking collectives  61.3 us (16%)
  matrix products  49.8 us (13%)
  local copies, waits for them, and re-layouts  27.3 us (7%)
  between operations  14.7 us (4%)
    another operation x3, other arithmetic, block_terms(): jax.scipy.linalg.solve_triangular(system, right_side, lower=True, unit_di...  119 us
    all_gather x1, waiting for transfers between devices, body(): lax.all_gather(stacked, ('sp', 'fs'), axis=0, tiled=True)  89.4 us
    all_gather x2, blocking collectives, entering_2(): lax.all_gather(a.astype(kind), axis)  31.8 us
    dot_general x4, matrix products, pair_terms(): jnp.einsum('hbtc,hbic->hbti', left, right, precision=lax.Precision.HIGHEST)  8.86 us
    all_to_all x1, blocking collectives, body(): lax.all_to_all(local_mix, 'tp', split_axis=0, concat_axis=1, tiled=True)  8.49 us
    unnamed x136, local copies, waits for them, and re-layouts  7.9 us
    dot_general x1, matrix products, body(): jnp.dot(normed, lax.all_gather(stacked, ('sp', 'fs'), axis=0, tiled=True)...  7.79 us
  transfers between devices with their start and end apart: 3, of which 1 were waited for; matrix products, arithmetic and copies ran while one was open for 51% of the time, Pallas kernels for 0%

commit v1 on v0

--- a/solution.py
+++ b/solution.py
@@ -1,6 +1,10 @@
+import functools
+
 import jax
 import jax.numpy as jnp
 from jax import lax
+from jax.experimental import pallas as pl
+from jax.experimental.pallas import tpu as pltpu
 from jax.sharding import PartitionSpec as P
 
 NORM_FLOOR = 0.1
@@ -231,9 +235,366 @@
     return mixed.astype(jnp.bfloat16).reshape(1, -1, width)
 
 
+def halves(array):
+    high = array.astype(jnp.bfloat16)
+    low = (array - high.astype(jnp.float32)).astype(jnp.bfloat16)
+    return (high, low)
+
+
+def product(left, right, dims=((1,), (0,))):
+    def one(a, b):
+        return lax.dot_general(a, b, (dims, ((), ())), preferred_element_type=jnp.float32)
+
+    return one(left[0], right[0]) + (one(left[0], right[1]) + one(left[1], right[0]))
+
+
+def mixer_kernel(
+    size,
+    span,
+    group,
+    proj_ref,
+    pace_ref,
+    base_ref,
+    correction_ref,
+    gain_ref,
+    taps_ref,
+    begin_ref,
+    out_ref,
+    local_ref,
+    map_ref,
+    carry_ref,
+    add_ref,
+    conv_ref,
+):
+    length = proj_ref.shape[0]
+    heads = begin_ref.shape[0]
+    wide = heads * size
+    blocks = length // span
+    kernel, channels = taps_ref.shape
+    f32 = jnp.float32
+    row = lax.broadcasted_iota(jnp.int32, (span, span), 0)
+    col = lax.broadcasted_iota(jnp.int32, (span, span), 1)
+    strict = (row > col).astype(f32)
+    weak = (row >= col).astype(f32)
+    masks = jnp.concatenate(
+        [jnp.concatenate([strict, strict], axis=1), jnp.concatenate([weak, weak], axis=1)], axis=0
+    )
+    eye = (row == col).astype(f32)
+    square = (
+        lax.broadcasted_iota(jnp.int32, (size, size), 0)
+        == lax.broadcasted_iota(jnp.int32, (size, size), 1)
+    ).astype(f32)
+    least = min(8, span)
+    same = (row // least == col // least).astype(f32)
+    merges = []
+    width = least
+    while width < span:
+        merges.append(
+            ((row // (2 * width) == col // (2 * width)) & (row // width != col // width)).astype(f32)
+        )
+        width = 2 * width
+    weak_bf = weak.astype(jnp.bfloat16)
+
+    def step(turn, _):
+        items = []
+        for part in range(group):
+            block = turn * group + part
+            rows = pl.ds(pl.multiple_of(block * span, span), span)
+            query = proj_ref[rows, 0:wide].astype(f32)
+            keys = proj_ref[rows, wide : 2 * wide].astype(f32)
+            values = proj_ref[rows, 2 * wide : 3 * wide].astype(f32)
+            decay_in = proj_ref[rows, 3 * wide : 4 * wide].astype(f32)
+            log_keep = -jnp.exp(base_ref[...] + jnp.tanh(decay_in)) * pace_ref[rows, :]
+            high = log_keep.astype(jnp.bfloat16)
+            rest = log_keep - high.astype(f32)
+            mid = rest.astype(jnp.bfloat16)
+            low = (rest - mid.astype(f32)).astype(jnp.bfloat16)
+            total = (
+                jnp.dot(weak_bf, high, preferred_element_type=f32)
+                + jnp.dot(weak_bf, mid, preferred_element_type=f32)
+                + jnp.dot(weak_bf, low, preferred_element_type=f32)
+            )
+            last = total[span - 1 : span, :]
+            lead = jnp.exp(total - log_keep)
+            grown = jnp.exp(total)
+            back = jnp.exp(-total)
+            tail = jnp.exp(last - total)
+            ended = jnp.exp(last)
+            for head in range(heads):
+                at = slice(head * size, (head + 1) * size)
+                key = keys[:, at]
+                unit = key * lax.rsqrt(
+                    jnp.maximum(jnp.sum(key * key, axis=1, keepdims=True), 1.0)
+                )
+                write = unit * correction_ref[:, at]
+                lead_remove = -unit * lead[:, at]
+                lead_query = query[:, at] * grown[:, at]
+                items.append(
+                    dict(
+                        at=(block, head),
+                        value=values[:, at],
+                        lead_remove=lead_remove,
+                        lead_query=lead_query,
+                        left=jnp.concatenate([lead_remove, lead_query], axis=0),
+                        right=jnp.concatenate([write * back[:, at], key * back[:, at]], axis=0),
+                        tail_write=write * tail[:, at],
+                        tail_key=key * tail[:, at],
+                        ended=ended[:, at],
+                    )
+                )
+        for item in items:
+            item["pair"] = (
+                product(halves(item["left"]), halves(item["right"]), ((1,), (1,))) * masks
+            )
+        for item in items:
+            item["system"] = item["pair"][:span, :span]
+            item["power"] = halves(item["system"] * same)
+            item["inverse"] = eye + item["system"] * same
+        width = 2
+        while width < least:
+            for item in items:
+                item["power"] = halves(product(item["power"], item["power"]))
+            for item in items:
+                item["inverse"] = item["inverse"] + product(
+                    halves(item["inverse"]), item["power"]
+                )
+            width = 2 * width
+        for item in items:
+            padded = jnp.concatenate([jnp.zeros_like(item["value"]), item["value"]], axis=0)
+            item["mixed"] = product(halves(item["pair"]), halves(padded))
+        for merge in merges:
+            for item in items:
+                item["inside"] = halves(item["inverse"])
+                item["next"] = halves(product(halves(item["system"] * merge), item["inside"]))
+            for item in items:
+                item["inverse"] = item["inverse"] + product(item["inside"], item["next"])
+        for item in items:
+            right_side = jnp.concatenate([item["mixed"][:span], item["lead_remove"]], axis=1)
+            item["solved"] = halves(product(halves(item["inverse"]), halves(right_side)))
+        for item in items:
+            block, head = item["at"]
+            seen = product(halves(item["pair"][span:, :span]), item["solved"])
+            local_ref[head, block] = seen[:, :size] + item["mixed"][span:]
+            map_ref[head, block] = item["lead_query"] + seen[:, size:]
+            carried = product(item["solved"], halves(item["tail_write"]), ((0,), (0,)))
+            carry_ref[head, block] = carried[size:] + square * item["ended"]
+            add_ref[head, block] = carried[:size] + product(
+                halves(item["value"]), halves(item["tail_key"]), ((0,), (0,))
+            )
+        return 0
+
+    lax.fori_loop(0, blocks // group, step, 0)
+
+    states = [begin_ref[head] for head in range(heads)]
+    for block in range(blocks):
+        rows = pl.ds(block * span, span)
+        gate = proj_ref[rows, 4 * wide : 5 * wide].astype(f32)
+        pieces = []
+        for head in range(heads):
+            at = slice(head * size, (head + 1) * size)
+            state = halves(states[head])
+            out = local_ref[head, block] + product(
+                halves(map_ref[head, block]), state, ((1,), (1,))
+            )
+            states[head] = product(state, halves(carry_ref[head, block])) + add_ref[head, block]
+            centered = out - jnp.mean(out, axis=1, keepdims=True)
+            variance = jnp.mean(centered * centered, axis=1, keepdims=True)
+            pieces.append(centered * lax.rsqrt(variance + GROUP_FLOOR))
+        grouped = jnp.concatenate(pieces, axis=1) * gain_ref[...]
+        out_ref[rows, 0:wide] = (grouped * gate * jax.nn.sigmoid(gate)).astype(out_ref.dtype)
+
+    lead_rows = conv_ref.shape[0] - length
+    conv_ref[0:lead_rows, :] = jnp.zeros((lead_rows, channels), f32)
+    conv_at = 5 * wide
+    for block in range(blocks):
+        rows = pl.ds(block * span, span)
+        value = proj_ref[rows, conv_at : conv_at + channels].astype(f32)
+        admit = proj_ref[rows, conv_at + channels : conv_at + 2 * channels].astype(f32)
+        conv_ref[pl.ds(lead_rows + block * span, span), :] = (
+            (value * jax.nn.sigmoid(admit)).astype(jnp.bfloat16).astype(f32)
+        )
+    for block in range(blocks):
+        total = jnp.zeros((span, channels), f32)
+        for place in range(kernel):
+            first = lead_rows - (kernel - 1) + block * span + place
+            total = total + taps_ref[place : place + 1, :] * conv_ref[pl.ds(first, span), :]
+        rows = pl.ds(block * span, span)
+        out_ref[rows, wide : wide + channels] = total.astype(out_ref.dtype)
+        out_ref[rows, wide + channels : wide + 2 * channels] = proj_ref[
+            rows, conv_at + 2 * channels : conv_at + 3 * channels
+        ]
+
+
+def mixer(projected, pace, base, correction, gain, taps, begin):
+    length = projected.shape[0]
+    heads, size, _ = begin.shape
+    kernel, channels = taps.shape
+    span = 64
+    blocks = length // span
+    group = next(n for n in (4, 3, 2, 1) if blocks % n == 0)
+    lead_rows = -(-(kernel - 1) // 8) * 8
+    maps = pltpu.VMEM((heads, blocks, size, size), jnp.float32)
+    return pl.pallas_call(
+        functools.partial(mixer_kernel, size, span, group),
+        out_shape=jax.ShapeDtypeStruct((length, heads * size + 2 * channels), jnp.bfloat16),
+        in_specs=[pl.BlockSpec(memory_space=pltpu.VMEM)] * 7,
+        out_specs=pl.BlockSpec(memory_space=pltpu.VMEM),
+        scratch_shapes=[
+            pltpu.VMEM((heads, blocks, span, size), jnp.float32),
+            pltpu.VMEM((heads, blocks, span, size), jnp.float32),
+            maps,
+            maps,
+            pltpu.VMEM((lead_rows + length, channels), jnp.float32),
+        ],
+        compiler_params=pltpu.CompilerParams(vmem_limit_bytes=48 * 1024 * 1024),
+        cost_estimate=pl.CostEstimate(
+            flops=60_000_000_000, bytes_accessed=4_000_000, transcendentals=0
+        ),
+        name="mixer",
+    )(projected, pace, base, correction, gain, taps, begin)
+
+
+def own_part(array, axis, count, dim):
+    part = array.shape[dim] // count
+    return lax.dynamic_slice_in_dim(array, lax.axis_index(axis) * part, part, dim)
+
+
+def whole_sequence_body(
+    tokens,
+    decay_pace,
+    start_state,
+    norm_gain,
+    conv_value,
+    conv_admit,
+    conv_gate,
+    state_query,
+    state_key,
+    state_value,
+    state_decay,
+    state_gate,
+    conv_taps,
+    conv_gain,
+    point_weight,
+    decay_base,
+    correction,
+    group_gain,
+    output_conv,
+    output_state,
+):
+    along = lax.axis_size("sp")
+    across = lax.axis_size("fs")
+    groups = lax.axis_size("tp")
+    width = tokens.shape[-1]
+    rows = tokens.reshape(-1, width)
+    depth = conv_value.shape[0]
+
+    shards = (
+        state_query,
+        state_key,
+        state_value,
+        state_decay,
+        state_gate,
+        conv_value,
+        conv_admit,
+        conv_gate,
+    )
+    parted = jnp.concatenate(
+        [shard.reshape(depth, along, -1).transpose(1, 0, 2) for shard in shards], axis=2
+    )
+    swapped = lax.all_to_all(parted, "sp", split_axis=0, concat_axis=0, tiled=True)
+    weights = lax.all_gather(swapped, "fs", axis=0).reshape(width, -1)
+
+    floats = rows.astype(jnp.float32)
+    inverse = lax.rsqrt(jnp.mean(floats * floats, axis=1, keepdims=True) + NORM_FLOOR)
+    normed = (floats * inverse * norm_gain).astype(jnp.bfloat16)
+    normed = (
+        normed.reshape(-1, along, across, depth).transpose(0, 2, 1, 3).reshape(rows.shape)
+    )
+    sequence = lax.all_gather(normed, "sp", axis=0, tiled=True)
+    projected = jnp.dot(sequence, weights, preferred_element_type=jnp.float32).astype(jnp.bfloat16)
+    pace = lax.all_gather(decay_pace.reshape(-1), "sp", axis=0, tiled=True)[:, None]
+
+    channels = conv_value.shape[1]
+    mixed_in = mixer(
+        projected,
+        pace,
+        own_part(decay_base[None], "sp", along, 1),
+        own_part(correction[None], "sp", along, 1),
+        own_part(group_gain[None], "sp", along, 1),
+        own_part(conv_taps, "sp", along, 1),
+        own_part(start_state[0], "sp", along, 0),
+    )
+    owners = along * groups
+    heads_wide = state_query.shape[1] // along
+    part = channels // along
+    sent = mixed_in.reshape(owners, -1, mixed_in.shape[1])
+    moved = lax.all_to_all(sent, ("sp", "tp"), split_axis=0, concat_axis=0, tiled=True)
+    own_rows = moved.shape[1]
+    moved = moved.reshape(along, groups, own_rows, -1).transpose(2, 1, 0, 3)
+    state_out = moved[..., :heads_wide].reshape(own_rows, groups, -1)
+    conv_sum = (
+        moved[..., heads_wide : heads_wide + part].reshape(own_rows, -1).astype(jnp.float32)
+    )
+    gate_conv = moved[..., heads_wide + part :].reshape(own_rows, -1).astype(jnp.float32)
+
+    columns = output_conv.shape[1]
+    local_rows = output_conv.shape[0] + output_state.shape[0]
+    gain_rows = conv_gain.astype(jnp.bfloat16).reshape(-1, columns)
+    spare = -gain_rows.shape[0] % 16
+    joined = lax.all_gather(
+        jnp.concatenate(
+            [
+                output_conv,
+                output_state,
+                gain_rows,
+                jnp.zeros((spare, columns), jnp.bfloat16),
+            ],
+            axis=0,
+        ),
+        "tp",
+        axis=0,
+    )
+    whole_gain = (
+        joined[:, local_rows : local_rows + gain_rows.shape[0]].reshape(-1).astype(jnp.float32)
+    )
+    output_rows = joined[:, :local_rows].reshape(-1, columns)
+    output_weights = lax.all_gather(output_rows, ("sp", "fs"), axis=1, tiled=True)
+
+    mean = jnp.mean(conv_sum, axis=1, keepdims=True)
+    spread = jnp.mean(conv_sum * conv_sum, axis=1, keepdims=True) - mean * mean
+    shaped = jax.nn.silu(
+        (conv_sum - mean) * lax.rsqrt(spread + CHANNEL_FLOOR) * whole_gain
+    ).astype(jnp.bfloat16)
+    pointwise = jnp.dot(shaped, point_weight, preferred_element_type=jnp.float32)
+    conv_out = (pointwise * jax.nn.silu(gate_conv)).astype(jnp.bfloat16)
+    joined_rows = jnp.concatenate(
+        [conv_out.reshape(own_rows, groups, -1), state_out], axis=2
+    ).reshape(own_rows, -1)
+    mixed = jnp.dot(joined_rows, output_weights, preferred_element_type=jnp.float32)
+    return mixed.astype(jnp.bfloat16).reshape(1, -1, width)
+
+
+def dispatch(*arrays):
+    along = lax.axis_size("sp")
+    tokens, start_state, conv_value, conv_gain, output_conv = (
+        arrays[0],
+        arrays[2],
+        arrays[4],
+        arrays[13],
+        arrays[18],
+    )
+    fits = (
+        start_state.shape[1] % along == 0
+        and (conv_value.shape[1] // along) % 64 == 0
+        and conv_gain.shape[0] % output_conv.shape[1] == 0
+        and (tokens.shape[1] * along) % 64 == 0
+    )
+    return (whole_sequence_body if fits else body)(*arrays)
+
+
 def solution(mesh):
     return jax.shard_map(
-        body,
+        dispatch,
         mesh=mesh,
         in_specs=(
             P("fs", "sp", None),

time: 377 us -> 208 us (0.55)
  other arithmetic: 128 us -> 2.29 us
  matrix products: 49.8 us -> 11.8 us
  Pallas kernels: 0 us -> 14.5 us
  local copies, waits for them, and re-layouts: 27.3 us -> 13.5 us
  waiting for transfers between devices: 89.4 us -> 77.5 us
  blocking collectives: 61.3 us -> 68.2 us
    another operation x6 -> x0, other arithmetic: 120 us -> none  [the longest x3 119 us: block_terms(): jax.scipy.linalg.solve_triangular(system, right_side, lower=True, unit_di...]
    all_gather x6 -> x1, blocking collectives: 52.8 us -> 6.38 us  [whole_sequence_body(): lax.all_gather(jnp.concatenate([output_conv, output_state, gain_rows, jnp...]
    all_to_all x1, blocking collectives: 8.49 us -> 49.2 us  [whole_sequence_body(): lax.all_to_all(parted, 'sp', split_axis=0, concat_axis=0, tiled=True)]
    dot_general x23 -> x3, matrix products: 48.2 us -> 11.8 us  [the longest x1 6.8 us: whole_sequence_body(): jnp.dot(sequence, weights, preferred_element_type=jnp.float32)]
    all_gather x2 -> x3, waiting for transfers between devices: 89.4 us -> 58.7 us  [the longest x1 30.7 us: whole_sequence_body(): weights = lax.all_gather(swapped, 'fs', axis=0).reshape(width, -1)]
    all_to_all x0 -> x1, waiting for transfers between devices: none -> 18.8 us  [whole_sequence_body(): lax.all_to_all(sent, ('sp', 'tp'), split_axis=0, concat_axis=0, tiled=True)]
    pallas_call x0 -> x1, Pallas kernels: none -> 14.5 us  [mixer(): pl.pallas_call(functools.partial(mixer_kernel, size, span, group), out_sh...]
    unnamed x0 -> x1, blocking collectives: none -> 12.6 us
  transfers between devices with their start and end apart: 3 -> 4, of which waited for: 1 -> 4; matrix products, arithmetic and copies ran while one was open for 51% -> 8% of each run, Pallas kernels for 0% -> 7%
where the time goes in v1:
time: 208 us
  waiting for transfers between devices  77.5 us (37%)
  blocking collectives  68.2 us (33%)
  Pallas kernels  14.5 us (7%)
  between operations  14.2 us (7%)
  local copies, waits for them, and re-layouts  13.5 us (6%)
  matrix products  11.8 us (6%)
  starting transfers between devices  5.6 us (3%)
  other arithmetic  2.29 us (1%)
    all_to_all x1, blocking collectives, whole_sequence_body(): lax.all_to_all(parted, 'sp', split_axis=0, concat_axis=0, tiled=True)  49.2 us
    all_gather x1, waiting for transfers between devices, whole_sequence_body(): weights = lax.all_gather(swapped, 'fs', axis=0).reshape(width, -1)  30.7 us
    all_gather x1, waiting for transfers between devices, whole_sequence_body(): lax.all_gather(output_rows, ('sp', 'fs'), axis=1, tiled=True)  22.6 us
    all_to_all x1, waiting for transfers between devices, whole_sequence_body(): lax.all_to_all(sent, ('sp', 'tp'), split_axis=0, concat_axis=0, tiled=True)  18.8 us
    pallas_call x1, Pallas kernels, mixer(): pl.pallas_call(functools.partial(mixer_kernel, size, span, group), out_sh...  14.5 us
    unnamed x1, blocking collectives  12.6 us
    dot_general x1, matrix products, whole_sequence_body(): jnp.dot(sequence, weights, preferred_element_type=jnp.float32)  6.8 us
    all_gather x1, blocking collectives, whole_sequence_body(): lax.all_gather(jnp.concatenate([output_conv, output_state, gain_rows, jnp...  6.38 us
  transfers between devices with their start and end apart: 4, of which 4 were waited for; matrix products, arithmetic and copies ran while one was open for 8% of the time, Pallas kernels for 7%

profile of v1, /device:TPU:0, one launch (start us, length us, event | category | flops | bytes accessed | tf_op | source)
XLA Modules:
  0.0 207.5 jit_solution(16939161022965089665)
XLA Ops:
  6.5 2.4 %reshape.138 = f32[192,4,4,128]{3,2,1,0:T(4,128)S(1)} reshape(bf16[1,192,2048]{2,1,0:T(8,128)(2,1)} %param.20) | data formatting | bytes 2359296 | tf_op jit(solution)/shard_map/convert_element_type | solution.py:507
  9.0 1.5 multiply_reduce_fusion
  10.4 0.5 fusion.10
  10.9 1.5 reshape.119
  12.7 0.1 copy.130
  13.2 1.0 copy.134
  14.2 0.9 copy.135
  15.5 49.2 %all_to_all.10 = bf16[4,128,832]{1,2,0:T(8,128)(2,1)} all-to-all(bf16[4,128,832]{1,2,0:T(8,128)(2,1)S(1)} %constant_dynamic-update-slice_fusion), channel_id=1, replica_groups=mesh['sp'=4,'fs'=4,'tp'=2] {'sp'}, dimensions={0} | all-to-all | bytes 1703936 | tf_op jit(solution)/shard_map/all_to_all | solution.py:504
  64.9 0.2 maximum_maximum_fusion
  65.1 6.4 %all-gather.2 = bf16[1568,128]{1,0:T(8,128)(2,1)S(1)} all-gather(bf16[784,128]{1,0:T(8,128)(2,1)S(1)} %maximum_maximum_fusion), channel_id=4, replica_groups=mesh['sp'=4,'fs'=4,'tp'=2] {'tp'}, dimensions={0}, use_global_device_ids=true | all-gather | bytes 602112 | tf_op jit(solution)/shard_map/all_gather | solution.py:544
  71.5 0.8 slice.24
  72.3 0.6 dynamic-slice.13
  73.5 0.2 dynamic-update-slice
  73.8 12.6 %all-reduce = f32[768]{0:T(1024)S(1)} all-reduce(f32[768]{0:T(1024)S(1)} %dynamic-update-slice), channel_id=3, replica_groups=mesh['sp'=4,'fs'=4,'tp'=2] {'sp'}, use_global_device_ids=true, to_apply=%add | all-reduce | flops 768 | bytes 6144
  86.4 0.2 broadcast_in_dim.6.pace_ref
  86.5 0.8 dynamic-slice_bitcast_fusion.3.base_ref
  87.3 0.8 dynamic-slice_bitcast_fusion.1
  88.1 0.8 dynamic-slice_bitcast_fusion.begin_ref
  89.0 5.4 %all-gather.7.cloned.1.call-done = bf16[768,2048]{1,0:T(8,128)(2,1)} async-done(((bf16[192,2048]{1,0:T(8,128)(2,1)}), bf16[768,2048]{1,0:T(8,128)(2,1)}) %all-gather.7.cloned.1.call-update) | async-done | bytes 3145744 | tf_op jit(solution)/shard_map/all_gather | solution.py:513
  94.4 30.7 %all-gather.11.cloned.1.call-done = bf16[16,128,832]{1,2,0:T(8,128)(2,1)} async-done(((bf16[4,128,832]{1,2,0:T(8,128)(2,1)}), bf16[16,128,832]{1,2,0:T(8,128)(2,1)}) %all-gather.11.cloned.1.call-update) | async-done | bytes 3407888 | tf_op jit(solution)/shard_map/all_gather | solution.py:505
  125.1 6.8 %fusion.4 = bf16[768,832]{0,1:T(8,128)(2,1)} fusion(bf16[768,2048]{1,0:T(8,128)(2,1)} %all-gather.7.cloned.1.call-done, bf16[16,128,832]{1,2,0:T(8,128)(2,1)} %all-gather.11.cloned.1.call-done), kind=kOutput, calls=%fused_computation.5 | convolution fusion | flops 2617884672 | bytes 7831552 | tf_op jit(solution)/shard_map/dot_general | solution.py:514
  131.9 1.8 copy.138.proj_ref
  133.7 14.5 %mixer.1 = bf16[768,256]{1,0:T(8,128)(2,1)} custom-call(bf16[768,832]{1,0:T(8,128)(2,1)S(1)} %copy.138.proj_ref, f32[768,1]{1,0:T(8,128)S(1)} %broadcast_in_dim.6.pace_ref, f32[1,128]{1,0:T(1,128)S(1)} %dynamic-slice_bitcast_fusion.3.base_ref, f32[1,128]{1,0:T(1,128)S(1)} %get-tuple-element.12.correction_ref, f32[1,128]{1,0:T(1,128)S(1)} %get-tuple-element.11.gain_ref, ...), custom_call_target="tpu_custom_call" | custom-call | flops 60000002048 | bytes 4000000 | tf_op jit(solution)/shard_map/mixer/pallas_call | solution.py:437
  148.1 5.5 %all-to-all-start.1 = ((bf16[8,96,256]{2,1,0:T(8,128)(2,1)}), bf16[8,96,256]{2,1,0:T(8,128)(2,1)S(1)}, u32[]{:S(2)}, u32[]{:S(2)}) async-start(bf16[8,96,256]{2,1,0:T(8,128)(2,1)} %bitcast.24), calls=%async_computation.1 | async-start | bytes 786432 | tf_op jit(solution)/shard_map/all_to_all | solution.py:531
  153.7 18.8 %all-to-all-done.1 = bf16[8,96,256]{2,1,0:T(8,128)(2,1)S(1)} async-done(((bf16[8,96,256]{2,1,0:T(8,128)(2,1)}), bf16[8,96,256]{2,1,0:T(8,128)(2,1)S(1)}, u32[]{:S(2)}, u32[]{:S(2)}) %all-to-all-start.1) | async-done | bytes 393248 | tf_op jit(solution)/shard_map/all_to_all | solution.py:531
  172.4 0.3 copy.140
  172.8 0.1 copy.147
  173.0 0.1 copy.143
  173.1 0.1 copy.141
  173.3 0.3 fusion.9
  173.7 22.6 %all-gather.9.cloned.1.call-done = bf16[1536,2048]{1,0:T(8,128)(2,1)} async-done(((bf16[1536,128]{1,0:T(8,128)(2,1)}), bf16[1536,2048]{1,0:T(8,128)(2,1)}) %all-gather.9.cloned.1.call-update) | async-done | bytes 6291472 | tf_op jit(solution)/shard_map/all_gather | solution.py:561
  196.3 4.7 %fusion.3 = bf16[1,96,2048]{2,1,0:T(8,128)(2,1)} fusion(bf16[96,1536]{1,0:T(8,128)(2,1)S(1)} %bitcast.80, bf16[1536,2048]{1,0:T(8,128)(2,1)} %all-gather.9.cloned.1.call-done), kind=kOutput, calls=%fused_computation.4 | convolution fusion | flops 604176384 | bytes 6979584 | tf_op jit(solution)/shard_map/dot_general | solution.py:573
  (64 shorter events, 1.3 us)
Async XLA Ops:
  6.5 166.8 %copy-start = (bf16[512,512]{1,0:T(8,128)(2,1)S(1)}, bf16[512,512]{1,0:T(8,128)(2,1)}, u32[]{:S(2)}) copy-start(bf16[512,512]{1,0:T(8,128)(2,1)} %param.34) | copy-start | bytes 1572868
  6.5 3.9 %copy-start.10 = (f32[2048]{0:T(1024)S(1)}, f32[2048]{0:T(1024)}, u32[]{:S(2)}) copy-start(f32[2048]{0:T(1024)} %param.23) | copy-start | bytes 24580
  6.5 87.9 %all-gather.7.cloned.1.call-start = ((), (), s32[]{:S(2)}) async-start(), calls=%async_computation.2 | async-start | bytes 3932160 | tf_op jit(solution)/shard_map/all_gather | solution.py:513
  8.9 3.6 %copy-start.1 = (bf16[128,512]{1,0:T(8,128)(2,1)S(1)}, bf16[128,512]{1,0:T(8,128)(2,1)}, u32[]{:S(2)}) copy-start(bf16[128,512]{1,0:T(8,128)(2,1)} %param.27) | copy-start | bytes 393220
  8.9 3.8 %copy-start.2 = (bf16[128,512]{1,0:T(8,128)(2,1)S(1)}, bf16[128,512]{1,0:T(8,128)(2,1)}, u32[]{:S(2)}) copy-start(bf16[128,512]{1,0:T(8,128)(2,1)} %param.28) | copy-start | bytes 393220
  8.9 3.9 %copy-start.3 = (bf16[128,512]{1,0:T(8,128)(2,1)S(1)}, bf16[128,512]{1,0:T(8,128)(2,1)}, u32[]{:S(2)}) copy-start(bf16[128,512]{1,0:T(8,128)(2,1)} %param.29) | copy-start | bytes 393220
  8.9 4.0 %copy-start.4 = (bf16[128,512]{1,0:T(8,128)(2,1)S(1)}, bf16[128,512]{1,0:T(8,128)(2,1)}, u32[]{:S(2)}) copy-start(bf16[128,512]{1,0:T(8,128)(2,1)} %param.30) | copy-start | bytes 393220
  9.0 4.1 %copy-start.5 = (bf16[128,512]{1,0:T(8,128)(2,1)S(1)}, bf16[128,512]{1,0:T(8,128)(2,1)}, u32[]{:S(2)}) copy-start(bf16[128,512]{1,0:T(8,128)(2,1)} %param.31) | copy-start | bytes 393220
  10.9 4.2 %copy-start.8 = (bf16[128,256]{1,0:T(8,128)(2,1)S(1)}, bf16[128,256]{1,0:T(8,128)(2,1)}, u32[]{:S(2)}) copy-start(bf16[128,256]{1,0:T(8,128)(2,1)} %param.26) | copy-start | bytes 196612
  12.4 52.4 %copy-start.12 = (f32[256]{0:T(256)S(1)}, f32[256]{0:T(256)}, u32[]{:S(2)}) copy-start(f32[256]{0:T(256)} %param.33) | copy-start | bytes 3076
  12.5 52.4 %copy-start.6 = (bf16[512,128]{1,0:T(8,128)(2,1)S(1)}, bf16[512,128]{1,0:T(8,128)(2,1)}, u32[]{:S(2)}) copy-start(bf16[512,128]{1,0:T(8,128)(2,1)} %param.39) | copy-start | bytes 393220
  12.5 52.4 %copy-start.7 = (bf16[256,128]{1,0:T(8,128)(2,1)S(1)}, bf16[256,128]{1,0:T(8,128)(2,1)}, u32[]{:S(2)}) copy-start(bf16[256,128]{1,0:T(8,128)(2,1)} %param.38) | copy-start | bytes 196612
  12.5 112.6 %all-gather.11.cloned.1.call-start = ((), (), s32[]{:S(2)}) async-start(), calls=%async_computation.4 | async-start | bytes 4259840 | tf_op jit(solution)/shard_map/all_gather | solution.py:505
  15.3 57.0 %copy-start.13 = (u32[32]{0:T(128)S(1)}, u32[32]{0:T(128)}, u32[]{:S(2)}) copy-start(u32[32]{0:T(128)} %constant.43) | copy-start | bytes 388
  15.3 58.2 %copy-start.11 = (f32[1,192]{1,0:T(1,128)S(1)}, f32[1,192]{1,0:T(1,128)}, u32[]{:S(2)}) copy-start(f32[1,192]{1,0:T(1,128)} %param.21) | copy-start | bytes 2308
  15.3 72.7 %copy-start.9 = (f32[31,256]{1,0:T(8,128)S(1)}, f32[31,256]{1,0:T(8,128)}, u32[]{:S(2)}) copy-start(f32[31,256]{1,0:T(8,128)} %param.32) | copy-start | bytes 95236
  64.7 131.6 %all-gather.9.cloned.1.call-start = ((), (), s32[]{:S(2)}) async-start(), calls=%async_computation.3 | async-start | bytes 6684672 | tf_op jit(solution)/shard_map/all_gather | solution.py:561
  148.1 24.3 %all-to-all-start.1 = ((bf16[8,96,256]{2,1,0:T(8,128)(2,1)}), bf16[8,96,256]{2,1,0:T(8,128)(2,1)S(1)}, u32[]{:S(2)}, u32[]{:S(2)}) async-start(bf16[8,96,256]{2,1,0:T(8,128)(2,1)} %bitcast.24), calls=%async_computation.1 | async-start | bytes 786432 | tf_op jit(solution)/shard_map/all_to_all | solution.py:531
Sparse Core Ops, SparseCore 0:
  12.6 81.7 all-gather.6
  95.9 29.0 all-gather.10
  127.2 69.0 all-gather.8

commit v2 on v1

--- a/solution.py
+++ b/solution.py
@@ -454,6 +454,195 @@
     )(projected, pace, base, correction, gain, taps, begin)
 
 
+def collect_kernel(
+    along,
+    normed_ref,
+    parted_ref,
+    pace_ref,
+    rows_ref,
+    proj_ref,
+    paces_ref,
+    joined_ref,
+    sequence,
+    weights,
+    w_send,
+    w_recv,
+    t_send,
+    t_recv,
+    p_send,
+    p_recv,
+    y_send,
+    y_recv,
+    c_send,
+    c_recv,
+    r_send,
+    r_recv,
+    x_send,
+    x_recv,
+    o_send,
+    o_recv,
+):
+    place = lax.axis_index("sp")
+    seat = lax.axis_index("fs")
+    side = lax.axis_index("tp")
+    depth = parted_ref.shape[1]
+    length = normed_ref.shape[0]
+    half = length // 2
+    near = seat + 1 - 2 * lax.rem(seat, 2)
+    far = lax.rem(seat + 2, 4)
+    other = 1 - side
+
+    def ahead(steps):
+        return lax.rem(place + steps, along)
+
+    def behind(steps):
+        return lax.rem(place + along - steps, along)
+
+    def block(sp_at, fs_at):
+        return weights.at[pl.ds(pl.multiple_of((sp_at * 4 + fs_at) * depth, depth), depth)]
+
+    def tokens_at(sp_at, side_at):
+        return sequence.at[
+            pl.ds(pl.multiple_of(sp_at * length + side_at * half, half), half)
+        ]
+
+    def send(source, target, send_sem, recv_sem, where):
+        copy = pltpu.make_async_remote_copy(
+            src_ref=source,
+            dst_ref=target,
+            send_sem=send_sem,
+            recv_sem=recv_sem,
+            device_id=where,
+            device_id_type=pl.DeviceIdType.MESH,
+        )
+        copy.start()
+        sent.append(copy)
+
+    def arrive(target, send_sem, recv_sem, where):
+        pltpu.make_async_remote_copy(
+            src_ref=target,
+            dst_ref=target,
+            send_sem=send_sem,
+            recv_sem=recv_sem,
+            device_id=where,
+            device_id_type=pl.DeviceIdType.MESH,
+        ).wait_recv()
+
+    sent = []
+    barrier = pltpu.get_barrier_semaphore()
+    partners = [{"sp": ahead(s)} for s in range(1, along)]
+    partners += [{"fs": near}, {"fs": far}, {"tp": other}]
+    for partner in partners:
+        pl.semaphore_signal(
+            barrier, inc=1, device_id=partner, device_id_type=pl.DeviceIdType.MESH
+        )
+    pl.semaphore_wait(barrier, len(partners))
+
+    order = sorted(range(1, along), key=lambda s: min(s, along - s))
+    own = parted_ref.at[place]
+    for s in order:
+        send(
+            parted_ref.at[ahead(s)], block(place, seat), w_send.at[s], w_recv.at[s], {"sp": ahead(s)}
+        )
+    send(own, block(place, seat), y_send.at[0], y_recv.at[0], {"fs": far})
+    send(own, block(place, seat), c_send.at[0], c_recv.at[0], {"fs": near})
+    for s in order:
+        send(pace_ref, paces_ref.at[place], p_send.at[s], p_recv.at[s], {"sp": ahead(s)})
+    for s in order:
+        send(
+            normed_ref.at[pl.ds(pl.multiple_of(side * half, half), half)],
+            tokens_at(place, side),
+            t_send.at[s],
+            t_recv.at[s],
+            {"sp": ahead(s)},
+        )
+    send(rows_ref, joined_ref.at[side], o_send.at[0], o_recv.at[0], {"tp": other})
+
+    block(place, seat)[...] = parted_ref[place]
+    sequence[pl.ds(pl.multiple_of(place * length, length), length), :] = normed_ref[...]
+    joined_ref[side] = rows_ref[...]
+    paces_ref[place] = pace_ref[...]
+
+    def weights_on(s):
+        here = block(behind(s), seat)
+        arrive(here, w_send.at[s], w_recv.at[s], {"sp": ahead(s)})
+        send(here, here, y_send.at[s], y_recv.at[s], {"fs": far})
+        send(here, here, c_send.at[s], c_recv.at[s], {"fs": near})
+
+    def relay(s):
+        here = block(behind(s), far)
+        arrive(here, y_send.at[s], y_recv.at[s], {"fs": far})
+        send(here, here, r_send.at[s], r_recv.at[s], {"fs": near})
+
+    def tokens_on(s):
+        here = tokens_at(behind(s), side)
+        arrive(here, t_send.at[s], t_recv.at[s], {"sp": ahead(s)})
+        send(here, here, x_send.at[s], x_recv.at[s], {"tp": other})
+
+    for s in order[:2]:
+        weights_on(s)
+    relay(0)
+    for s in order[2:]:
+        weights_on(s)
+    for at, s in enumerate(order):
+        relay(s)
+        tokens_on(s)
+
+    for s in [0] + order:
+        arrive(block(behind(s), near), c_send.at[s], c_recv.at[s], {"fs": near})
+        beyond = lax.rem(near + 2, 4)
+        arrive(block(behind(s), beyond), r_send.at[s], r_recv.at[s], {"fs": near})
+    for s in order:
+        arrive(tokens_at(behind(s), other), x_send.at[s], x_recv.at[s], {"tp": other})
+        arrive(paces_ref.at[behind(s)], p_send.at[s], p_recv.at[s], {"sp": ahead(s)})
+    arrive(joined_ref.at[other], o_send.at[0], o_recv.at[0], {"tp": other})
+    for copy in sent:
+        copy.wait_send()
+
+    total = sequence.shape[0]
+    tile = next(n for n in (256, 192, 128, 96, 64, 32, 16) if total % n == 0)
+
+    def multiply(turn, _):
+        at = pl.ds(pl.multiple_of(turn * tile, tile), tile)
+        proj_ref[at, :] = jnp.dot(
+            sequence[at, :], weights[...], preferred_element_type=jnp.float32
+        ).astype(proj_ref.dtype)
+        return 0
+
+    lax.fori_loop(0, total // tile, multiply, 0)
+
+
+def collect(normed, parted, pace, rows):
+    along = parted.shape[0]
+    length, width = normed.shape
+    columns = parted.shape[2]
+    pair = pltpu.SemaphoreType.DMA((along,))
+    single = pltpu.SemaphoreType.DMA((1,))
+    return pl.pallas_call(
+        functools.partial(collect_kernel, along),
+        out_shape=(
+            jax.ShapeDtypeStruct((along * length, columns), jnp.bfloat16),
+            jax.ShapeDtypeStruct((along,) + pace.shape, pace.dtype),
+            jax.ShapeDtypeStruct((2,) + rows.shape, rows.dtype),
+        ),
+        in_specs=[pl.BlockSpec(memory_space=pltpu.VMEM)] * 4,
+        out_specs=(pl.BlockSpec(memory_space=pltpu.VMEM),) * 3,
+        scratch_shapes=[
+            pltpu.VMEM((along * length, width), jnp.bfloat16),
+            pltpu.VMEM((width, columns), jnp.bfloat16),
+        ]
+        + [pair] * 14
+        + [single] * 2,
+        compiler_params=pltpu.CompilerParams(
+            collective_id=0, has_side_effects=True, vmem_limit_bytes=48 * 1024 * 1024
+        ),
+        cost_estimate=pl.CostEstimate(
+            flops=60_000_000_000, bytes_accessed=8_000_000, transcendentals=0
+        ),
+        name="collect",
+    )(normed, parted, pace, rows)
+
+
 def own_part(array, axis, count, dim):
     part = array.shape[dim] // count
     return lax.dynamic_slice_in_dim(array, lax.axis_index(axis) * part, part, dim)
@@ -482,7 +671,6 @@
     output_state,
 ):
     along = lax.axis_size("sp")
-    across = lax.axis_size("fs")
     groups = lax.axis_size("tp")
     width = tokens.shape[-1]
     rows = tokens.reshape(-1, width)
@@ -501,18 +689,23 @@
     parted = jnp.concatenate(
         [shard.reshape(depth, along, -1).transpose(1, 0, 2) for shard in shards], axis=2
     )
-    swapped = lax.all_to_all(parted, "sp", split_axis=0, concat_axis=0, tiled=True)
-    weights = lax.all_gather(swapped, "fs", axis=0).reshape(width, -1)
-
     floats = rows.astype(jnp.float32)
     inverse = lax.rsqrt(jnp.mean(floats * floats, axis=1, keepdims=True) + NORM_FLOOR)
     normed = (floats * inverse * norm_gain).astype(jnp.bfloat16)
-    normed = (
-        normed.reshape(-1, along, across, depth).transpose(0, 2, 1, 3).reshape(rows.shape)
-    )
-    sequence = lax.all_gather(normed, "sp", axis=0, tiled=True)
-    projected = jnp.dot(sequence, weights, preferred_element_type=jnp.float32).astype(jnp.bfloat16)
-    pace = lax.all_gather(decay_pace.reshape(-1), "sp", axis=0, tiled=True)[:, None]
+    columns = output_conv.shape[1]
+    local_rows = output_conv.shape[0] + output_state.shape[0]
+    gain_rows = conv_gain.astype(jnp.bfloat16).reshape(-1, columns)
+    spare = -gain_rows.shape[0] % 16
+    sent_rows = jnp.concatenate(
+        [output_conv, output_state, gain_rows, jnp.zeros((spare, columns), jnp.bfloat16)], axis=0
+    )
+    span = rows.shape[0]
+    lanes = -(-span // 128) * 128
+    sent_pace = jnp.broadcast_to(
+        jnp.pad(decay_pace.reshape(1, -1), ((0, 0), (0, lanes - span))), (8, lanes)
+    )
+    projected, paces, joined = collect(normed, parted, sent_pace, sent_rows)
+    pace = paces[:, 0, :span].reshape(-1, 1)
 
     channels = conv_value.shape[1]
     mixed_in = mixer(
@@ -537,23 +730,6 @@
     )
     gate_conv = moved[..., heads_wide + part :].reshape(own_rows, -1).astype(jnp.float32)
 
-    columns = output_conv.shape[1]
-    local_rows = output_conv.shape[0] + output_state.shape[0]
-    gain_rows = conv_gain.astype(jnp.bfloat16).reshape(-1, columns)
-    spare = -gain_rows.shape[0] % 16
-    joined = lax.all_gather(
-        jnp.concatenate(
-            [
-                output_conv,
-                output_state,
-                gain_rows,
-                jnp.zeros((spare, columns), jnp.bfloat16),
-            ],
-            axis=0,
-        ),
-        "tp",
-        axis=0,
-    )
     whole_gain = (
         joined[:, local_rows : local_rows + gain_rows.shape[0]].reshape(-1).astype(jnp.float32)
     )
@@ -584,7 +760,11 @@
         arrays[18],
     )
     fits = (
-        start_state.shape[1] % along == 0
+        along > 2
+        and lax.axis_size("fs") == 4
+        and lax.axis_size("tp") == 2
+        and tokens.shape[1] % 32 == 0
+        and start_state.shape[1] % along == 0
         and (conv_value.shape[1] // along) % 64 == 0
         and conv_gain.shape[0] % output_conv.shape[1] == 0
         and (tokens.shape[1] * along) % 64 == 0

time: 208 us -> 178 us (0.86)
  Pallas kernels: 14.5 us -> 88.7 us
  blocking collectives: 68.2 us -> 0 us
  waiting for transfers between devices: 77.5 us -> 46.4 us
  matrix products: 11.8 us -> 4.98 us
  starting transfers between devices: 5.6 us -> 11.1 us
    pallas_call x0 -> x1, Pallas kernels: none -> 74.3 us  [collect(): pl.pallas_call(functools.partial(collect_kernel, along), out_shape=(jax.S...]
    all_to_all x1 -> x0, blocking collectives: 49.2 us -> none  [whole_sequence_body(): lax.all_to_all(parted, 'sp', split_axis=0, concat_axis=0, tiled=True)]
    all_gather x2 -> x0, waiting for transfers between devices: 36.1 us -> none  [the longest x1 30.7 us: whole_sequence_body(): weights = lax.all_gather(swapped, 'fs', axis=0).reshape(width, -1)]
    unnamed x1 -> x0, blocking collectives: 12.6 us -> none
    all_gather x1, waiting for transfers between devices: 22.6 us -> 33.6 us  [whole_sequence_body(): lax.all_gather(output_rows, ('sp', 'fs'), axis=1, tiled=True)]
    dot_general x1 -> x0, matrix products: 6.8 us -> none  [whole_sequence_body(): jnp.dot(sequence, weights, preferred_element_type=jnp.float32)]
    all_gather x1 -> x0, blocking collectives: 6.38 us -> none  [whole_sequence_body(): lax.all_gather(jnp.concatenate([output_conv, output_state, gain_rows, jnp...]
    all_to_all x1, waiting for transfers between devices: 18.8 us -> 12.8 us  [whole_sequence_body(): lax.all_to_all(sent, ('sp', 'tp'), split_axis=0, concat_axis=0, tiled=True)]
  transfers between devices with their start and end apart: 4 -> 2, of which waited for: 4 -> 2; matrix products, arithmetic and copies ran while one was open for 8% -> 2% of each run, Pallas kernels for 7% -> 8%
where the time goes in v2:
time: 178 us
  Pallas kernels  88.7 us (50%)
  waiting for transfers between devices  46.4 us (26%)
  between operations  13.8 us (8%)
  local copies, waits for them, and re-layouts  12 us (7%)
  starting transfers between devices  11.1 us (6%)
  matrix products  4.98 us (3%)
    pallas_call x1, Pallas kernels, collect(): pl.pallas_call(functools.partial(collect_kernel, along), out_shape=(jax.S...  74.3 us
    all_gather x1, waiting for transfers between devices, whole_sequence_body(): lax.all_gather(output_rows, ('sp', 'fs'), axis=1, tiled=True)  33.6 us
    pallas_call x1, Pallas kernels, mixer(): pl.pallas_call(functools.partial(mixer_kernel, size, span, group), out_sh...  14.4 us
    all_to_all x1, waiting for transfers between devices, whole_sequence_body(): lax.all_to_all(sent, ('sp', 'tp'), split_axis=0, concat_axis=0, tiled=True)  12.8 us
    all_to_all x1, starting transfers between devices, whole_sequence_body(): lax.all_to_all(sent, ('sp', 'tp'), split_axis=0, concat_axis=0, tiled=True)  11.1 us
    unnamed x38, local copies, waits for them, and re-layouts  6.26 us
    dot_general x1, matrix products, whole_sequence_body(): jnp.dot(joined_rows, output_weights, preferred_element_type=jnp.float32)  4.66 us
  transfers between devices with their start and end apart: 2, of which 2 were waited for; matrix products, arithmetic and copies ran while one was open for 2% of the time, Pallas kernels for 8%

profile of v2, /device:TPU:0, one launch (start us, length us, event | category | flops | bytes accessed | tf_op | source)
XLA Modules:
  0.0 177.8 jit_solution(13717775715522903449)
XLA Ops:
  6.6 1.1 copy.122
  7.7 0.1 copy.123
  7.9 1.1 copy.114
  9.0 0.1 copy.115
  9.1 1.0 copy.116
  10.1 0.1 copy.117
  10.4 0.1 copy.119
  10.7 0.1 copy.121
  11.0 0.1 copy.125
  11.3 0.1 copy.127
  11.5 0.1 copy.129
  11.7 0.2 fusion.1
  11.9 0.3 fusion.3.normed_ref
  12.3 0.2 maximum_maximum_fusion.rows_ref
  12.5 0.4 concatenate.9.parted_ref
  12.9 74.3 %collect.1 = (bf16[768,832]{1,0:T(8,128)(2,1)S(1)}, f32[4,8,256]{2,1,0:T(8,128)S(1)}, bf16[2,784,128]{2,1,0:T(8,128)(2,1)S(1)}) custom-call(bf16[192,2048]{1,0:T(8,128)(2,1)S(1)} %fusion.3.normed_ref, bf16[4,128,832]{2,1,0:T(8,128)(2,1)S(1)} %concatenate.9.parted_ref, f32[8,256]{1,0:T(8,128)S(1)} %broadcast_in_dim.7.pace_ref, ...), custom_call_target="tpu_custom_call" | custom-call | flops 60000002048 | bytes 8000000 | tf_op jit(solution)/shard_map/collect/pallas_call | solution.py:621
  87.2 1.1 copy-done.1
  88.3 0.8 slice.23
  89.1 0.3 reshape_squeeze.4.pace_ref
  89.4 0.8 dynamic-slice_bitcast_fusion.3.base_ref
  90.2 0.8 dynamic-slice_bitcast_fusion.1
  91.0 0.8 dynamic-slice_bitcast_fusion.begin_ref
  91.8 1.3 copy-done.2
  93.2 14.4 %mixer.1 = bf16[768,256]{1,0:T(8,128)(2,1)} custom-call(bf16[768,832]{1,0:T(8,128)(2,1)S(1)} %copy-done.2, f32[768,1]{1,0:T(8,128)S(1)} %reshape_squeeze.4.pace_ref, f32[1,128]{1,0:T(1,128)S(1)} %dynamic-slice_bitcast_fusion.3.base_ref, f32[1,128]{1,0:T(1,128)S(1)} %get-tuple-element.18.correction_ref, f32[1,128]{1,0:T(1,128)S(1)} %get-tuple-element.17.gain_ref, ...), custom_call_target="tpu_custom_call" | custom-call | flops 60000002048 | bytes 4000000 | tf_op jit(solution)/shard_map/mixer/pallas_call | solution.py:437
  107.6 11.1 %all-to-all-start = ((bf16[8,96,256]{2,1,0:T(8,128)(2,1)}), bf16[8,96,256]{2,1,0:T(8,128)(2,1)S(1)}, u32[]{:S(2)}, u32[]{:S(2)}) async-start(bf16[8,96,256]{2,1,0:T(8,128)(2,1)} %bitcast.24), calls=%async_computation | async-start | bytes 786432 | tf_op jit(solution)/shard_map/all_to_all | solution.py:724
  118.7 12.8 %all-to-all-done = bf16[8,96,256]{2,1,0:T(8,128)(2,1)S(1)} async-done(((bf16[8,96,256]{2,1,0:T(8,128)(2,1)}), bf16[8,96,256]{2,1,0:T(8,128)(2,1)S(1)}, u32[]{:S(2)}, u32[]{:S(2)}) %all-to-all-start) | async-done | bytes 393248 | tf_op jit(solution)/shard_map/all_to_all | solution.py:724
  131.5 0.3 copy.131
  131.9 0.1 copy.134
  132.2 0.3 fusion.4
  132.6 0.1 copy.138
  132.8 33.6 %all-gather.2.cloned.1.call-done = bf16[1536,2048]{1,0:T(8,128)(2,1)} async-done(((bf16[1536,128]{1,0:T(8,128)(2,1)}), bf16[1536,2048]{1,0:T(8,128)(2,1)}) %all-gather.2.cloned.1.call-update) | async-done | bytes 6291472 | tf_op jit(solution)/shard_map/all_gather | solution.py:737
  166.3 4.7 %fusion = bf16[1,96,2048]{2,1,0:T(8,128)(2,1)} fusion(bf16[96,1536]{1,0:T(8,128)(2,1)S(1)} %bitcast.59, bf16[1536,2048]{1,0:T(8,128)(2,1)} %all-gather.2.cloned.1.call-done), kind=kOutput, calls=%fused_computation.1 | convolution fusion | flops 604176384 | bytes 6979584 | tf_op jit(solution)/shard_map/dot_general | solution.py:749
  (54 shorter events, 1.2 us)
Async XLA Ops:
  6.5 125.7 %copy-start = (bf16[512,512]{1,0:T(8,128)(2,1)S(1)}, bf16[512,512]{1,0:T(8,128)(2,1)}, u32[]{:S(2)}) copy-start(bf16[512,512]{1,0:T(8,128)(2,1)} %param.34) | copy-start | bytes 1572868
  6.5 3.8 %copy-start.4 = (bf16[128,512]{1,0:T(8,128)(2,1)S(1)}, bf16[128,512]{1,0:T(8,128)(2,1)}, u32[]{:S(2)}) copy-start(bf16[128,512]{1,0:T(8,128)(2,1)} %param.29) | copy-start | bytes 393220
  6.5 4.0 %copy-start.5 = (bf16[128,512]{1,0:T(8,128)(2,1)S(1)}, bf16[128,512]{1,0:T(8,128)(2,1)}, u32[]{:S(2)}) copy-start(bf16[128,512]{1,0:T(8,128)(2,1)} %param.30) | copy-start | bytes 393220
  6.5 4.3 %copy-start.8 = (bf16[128,256]{1,0:T(8,128)(2,1)S(1)}, bf16[128,256]{1,0:T(8,128)(2,1)}, u32[]{:S(2)}) copy-start(bf16[128,256]{1,0:T(8,128)(2,1)} %param.24) | copy-start | bytes 196612
  6.5 4.6 %copy-start.9 = (bf16[128,256]{1,0:T(8,128)(2,1)S(1)}, bf16[128,256]{1,0:T(8,128)(2,1)}, u32[]{:S(2)}) copy-start(bf16[128,256]{1,0:T(8,128)(2,1)} %param.25) | copy-start | bytes 196612
  6.5 159.8 %all-gather.2.cloned.1.call-start = ((), (), s32[]{:S(2)}) async-start(), calls=%async_computation.1 | async-start | bytes 6684672 | tf_op jit(solution)/shard_map/all_gather | solution.py:737
  7.7 3.7 %copy-start.10 = (bf16[128,256]{1,0:T(8,128)(2,1)S(1)}, bf16[128,256]{1,0:T(8,128)(2,1)}, u32[]{:S(2)}) copy-start(bf16[128,256]{1,0:T(8,128)(2,1)} %param.26) | copy-start | bytes 196612
  7.8 3.8 %copy-start.3 = (bf16[1,192,2048]{2,1,0:T(8,128)(2,1)S(1)}, bf16[1,192,2048]{2,1,0:T(8,128)(2,1)}, u32[]{:S(2)}) copy-start(bf16[1,192,2048]{2,1,0:T(8,128)(2,1)} %param.20) | copy-start | bytes 2359300
  10.1 1.8 %copy-start.14 = (f32[256]{0:T(256)S(1)}, f32[256]{0:T(256)}, u32[]{:S(2)}) copy-start(f32[256]{0:T(256)} %param.33) | copy-start | bytes 3076
  10.1 1.8 %copy-start.11 = (f32[2048]{0:T(1024)S(1)}, f32[2048]{0:T(1024)}, u32[]{:S(2)}) copy-start(f32[2048]{0:T(1024)} %param.23) | copy-start | bytes 24580
  11.0 1.3 copy-start.13
  11.0 1.3 copy-start.6
  11.0 1.3 copy-start.7
  87.2 1.1 copy-start.1
  88.3 2.6 %copy-start.12 = (f32[31,256]{1,0:T(8,128)S(1)}, f32[31,256]{1,0:T(8,128)}, u32[]{:S(2)}) copy-start(f32[31,256]{1,0:T(8,128)} %param.32) | copy-start | bytes 95236
  91.8 1.3 copy-start.2
  107.6 23.9 %all-to-all-start = ((bf16[8,96,256]{2,1,0:T(8,128)(2,1)}), bf16[8,96,256]{2,1,0:T(8,128)(2,1)S(1)}, u32[]{:S(2)}, u32[]{:S(2)}) async-start(bf16[8,96,256]{2,1,0:T(8,128)(2,1)} %bitcast.24), calls=%async_computation | async-start | bytes 786432 | tf_op jit(solution)/shard_map/all_to_all | solution.py:724
Sparse Core Ops, SparseCore 0:
  89.2 77.0 all-gather.1

commit v3 on v2

--- a/solution.py
+++ b/solution.py
@@ -692,12 +692,14 @@
     floats = rows.astype(jnp.float32)
     inverse = lax.rsqrt(jnp.mean(floats * floats, axis=1, keepdims=True) + NORM_FLOOR)
     normed = (floats * inverse * norm_gain).astype(jnp.bfloat16)
+    output_weights = lax.all_gather(
+        jnp.concatenate([output_conv, output_state], axis=0), ("sp", "fs"), axis=1, tiled=True
+    )
     columns = output_conv.shape[1]
-    local_rows = output_conv.shape[0] + output_state.shape[0]
     gain_rows = conv_gain.astype(jnp.bfloat16).reshape(-1, columns)
     spare = -gain_rows.shape[0] % 16
     sent_rows = jnp.concatenate(
-        [output_conv, output_state, gain_rows, jnp.zeros((spare, columns), jnp.bfloat16)], axis=0
+        [gain_rows, jnp.zeros((spare, columns), jnp.bfloat16)], axis=0
     )
     span = rows.shape[0]
     lanes = -(-span // 128) * 128
@@ -730,11 +732,7 @@
     )
     gate_conv = moved[..., heads_wide + part :].reshape(own_rows, -1).astype(jnp.float32)
 
-    whole_gain = (
-        joined[:, local_rows : local_rows + gain_rows.shape[0]].reshape(-1).astype(jnp.float32)
-    )
-    output_rows = joined[:, :local_rows].reshape(-1, columns)
-    output_weights = lax.all_gather(output_rows, ("sp", "fs"), axis=1, tiled=True)
+    whole_gain = joined[:, : gain_rows.shape[0]].reshape(-1).astype(jnp.float32)
 
     mean = jnp.mean(conv_sum, axis=1, keepdims=True)
     spread = jnp.mean(conv_sum * conv_sum, axis=1, keepdims=True) - mean * mean
@@ -744,9 +742,20 @@
     pointwise = jnp.dot(shaped, point_weight, preferred_element_type=jnp.float32)
     conv_out = (pointwise * jax.nn.silu(gate_conv)).astype(jnp.bfloat16)
     joined_rows = jnp.concatenate(
-        [conv_out.reshape(own_rows, groups, -1), state_out], axis=2
-    ).reshape(own_rows, -1)
-    mixed = jnp.dot(joined_rows, output_weights, preferred_element_type=jnp.float32)
+        [
+            conv_out.reshape(own_rows, groups, -1).transpose(1, 0, 2),
+            state_out.reshape(own_rows, groups, -1).transpose(1, 0, 2),
+        ],
+        axis=2,
+    )
+    traded = lax.all_to_all(joined_rows, "tp", split_axis=0, concat_axis=0, tiled=True)
+    partial = jnp.dot(
+        traded.reshape(groups * own_rows, -1), output_weights, preferred_element_type=jnp.float32
+    ).astype(jnp.bfloat16)
+    parts = lax.all_to_all(
+        partial.reshape(groups, own_rows, width), "tp", split_axis=0, concat_axis=0, tiled=True
+    )
+    mixed = jnp.sum(parts.astype(jnp.float32), axis=0)
     return mixed.astype(jnp.bfloat16).reshape(1, -1, width)
 
 

time: 178 us -> 171 us (0.961)
  waiting for transfers between devices: 46.4 us -> 9.2 us
  Pallas kernels: 88.7 us -> 108 us
  blocking collectives: 0 us -> 18.1 us
  starting transfers between devices: 11.1 us -> 5.67 us
  other arithmetic: 0.85 us -> 3.35 us
  matrix products: 4.98 us -> 2.99 us
  local copies, waits for them, and re-layouts: 12 us -> 10.2 us
    all_gather x1, waiting for transfers between devices: 33.6 us -> 0.01 us  [whole_sequence_body(): lax.all_gather(jnp.concatenate([output_conv, output_state], axis=0), ('sp...]
    pallas_call x1, Pallas kernels: 74.3 us -> 93.3 us  [collect(): pl.pallas_call(functools.partial(collect_kernel, along), out_shape=(jax.S...]
    all_to_all x0 -> x2, blocking collectives: none -> 18.1 us  [the longest x1 10.4 us: whole_sequence_body(): lax.all_to_all(partial.reshape(groups, own_rows, width), 'tp', split_axis...]
    all_to_all x1, starting transfers between devices: 11.1 us -> 5.63 us  [whole_sequence_body(): lax.all_to_all(sent, ('sp', 'tp'), split_axis=0, concat_axis=0, tiled=True)]
    all_to_all x1, waiting for transfers between devices: 12.8 us -> 9.19 us  [whole_sequence_body(): lax.all_to_all(sent, ('sp', 'tp'), split_axis=0, concat_axis=0, tiled=True)]
    dot_general x1, matrix products: 4.66 us -> 2.67 us  [whole_sequence_body(): jnp.dot(traded.reshape(groups * own_rows, -1), output_weights, preferred_...]
    unnamed x38 -> x36, local copies, waits for them, and re-layouts: 6.26 us -> 5.29 us
  transfers between devices with their start and end apart: 2 -> 2, of which waited for: 2 -> 1; matrix products, arithmetic and copies ran while one was open for 2% -> 5% of each run, Pallas kernels for 8% -> 63%
where the time goes in v3:
time: 171 us
  Pallas kernels  108 us (63%)
  blocking collectives  18.1 us (11%)
  between operations  13.8 us (8%)
  local copies, waits for them, and re-layouts  10.2 us (6%)
  waiting for transfers between devices  9.2 us (5%)
  starting transfers between devices  5.67 us (3%)
  other arithmetic  3.35 us (2%)
  matrix products  2.99 us (2%)
    pallas_call x1, Pallas kernels, collect(): pl.pallas_call(functools.partial(collect_kernel, along), out_shape=(jax.S...  93.3 us
    pallas_call x1, Pallas kernels, mixer(): pl.pallas_call(functools.partial(mixer_kernel, size, span, group), out_sh...  14.3 us
    all_to_all x1, blocking collectives, whole_sequence_body(): lax.all_to_all(partial.reshape(groups, own_rows, width), 'tp', split_axis...  10.4 us
    all_to_all x1, waiting for transfers between devices, whole_sequence_body(): lax.all_to_all(sent, ('sp', 'tp'), split_axis=0, concat_axis=0, tiled=True)  9.19 us
    all_to_all x1, blocking collectives, whole_sequence_body(): lax.all_to_all(joined_rows, 'tp', split_axis=0, concat_axis=0, tiled=True)  7.72 us
    all_to_all x1, starting transfers between devices, whole_sequence_body(): lax.all_to_all(sent, ('sp', 'tp'), split_axis=0, concat_axis=0, tiled=True)  5.63 us
    unnamed x36, local copies, waits for them, and re-layouts  5.29 us
  transfers between devices with their start and end apart: 2, of which 1 were waited for; matrix products, arithmetic and copies ran while one was open for 5% of the time, Pallas kernels for 63%

profile of v3, /device:TPU:0, one launch (start us, length us, event | category | flops | bytes accessed | tf_op | source)
XLA Modules:
  0.0 170.9 jit_solution(5790963834134935699)
XLA Ops:
  6.6 1.7 pad_maximum_fusion.1
  8.3 1.0 copy.99
  9.3 0.1 copy.100
  9.5 1.1 copy.91
  10.6 0.1 copy.92
  10.9 0.1 copy.94
  11.2 0.1 copy.96
  11.4 0.1 copy.98
  11.6 0.1 copy.101
  11.7 0.1 copy.102
  12.0 0.1 copy.104
  12.2 0.1 copy.106
  12.4 0.2 fusion
  12.7 0.3 fusion.2.normed_ref
  13.0 0.4 concatenate.12.parted_ref
  13.4 93.3 %collect.1 = (bf16[768,832]{1,0:T(8,128)(2,1)S(1)}, f32[4,8,256]{2,1,0:T(8,128)S(1)}, bf16[2,16,128]{2,1,0:T(8,128)(2,1)S(1)}) custom-call(bf16[192,2048]{1,0:T(8,128)(2,1)S(1)} %fusion.2.normed_ref, bf16[4,128,832]{2,1,0:T(8,128)(2,1)S(1)} %concatenate.12.parted_ref, f32[8,256]{1,0:T(8,128)S(1)} %broadcast_in_dim.5.pace_ref, ...), custom_call_target="tpu_custom_call" | custom-call | flops 60000002048 | bytes 8000000 | tf_op jit(solution)/shard_map/collect/pallas_call | solution.py:621
  106.6 1.1 copy-done.1
  107.7 0.3 reshape_squeeze.4.pace_ref
  108.0 0.8 dynamic-slice_bitcast_fusion.3.base_ref
  108.8 0.8 dynamic-slice_bitcast_fusion.1
  109.6 0.8 dynamic-slice_bitcast_fusion.begin_ref
  110.5 1.3 copy-done.2
  111.8 14.3 %mixer.1 = bf16[768,256]{1,0:T(8,128)(2,1)} custom-call(bf16[768,832]{1,0:T(8,128)(2,1)S(1)} %copy-done.2, f32[768,1]{1,0:T(8,128)S(1)} %reshape_squeeze.4.pace_ref, f32[1,128]{1,0:T(1,128)S(1)} %dynamic-slice_bitcast_fusion.3.base_ref, f32[1,128]{1,0:T(1,128)S(1)} %get-tuple-element.18.correction_ref, f32[1,128]{1,0:T(1,128)S(1)} %get-tuple-element.17.gain_ref, ...), custom_call_target="tpu_custom_call" | custom-call | flops 60000002048 | bytes 4000000 | tf_op jit(solution)/shard_map/mixer/pallas_call | solution.py:437
  126.1 5.6 %all-to-all-start = ((bf16[8,96,256]{2,1,0:T(8,128)(2,1)}), bf16[8,96,256]{2,1,0:T(8,128)(2,1)S(1)}, u32[]{:S(2)}, u32[]{:S(2)}) async-start(bf16[8,96,256]{2,1,0:T(8,128)(2,1)} %bitcast.24), calls=%async_computation | async-start | bytes 786432 | tf_op jit(solution)/shard_map/all_to_all | solution.py:726
  131.8 9.2 %all-to-all-done = bf16[8,96,256]{2,1,0:T(8,128)(2,1)S(1)} async-done(((bf16[8,96,256]{2,1,0:T(8,128)(2,1)}), bf16[8,96,256]{2,1,0:T(8,128)(2,1)S(1)}, u32[]{:S(2)}, u32[]{:S(2)}) %all-to-all-start) | async-done | bytes 393248 | tf_op jit(solution)/shard_map/all_to_all | solution.py:726
  140.9 0.3 copy.108
  141.7 0.3 fusion.3
  142.0 0.1 copy.114
  142.2 7.7 %all_to_all.15 = bf16[2,96,768]{2,1,0:T(8,128)(2,1)S(1)} all-to-all(bf16[2,96,768]{2,1,0:T(8,128)(2,1)S(1)} %pad_maximum_fusion), channel_id=1, replica_groups=mesh['sp'=4,'fs'=4,'tp'=2] {'tp'}, dimensions={0} | all-to-all | bytes 589824 | tf_op jit(solution)/shard_map/all_to_all | solution.py:751
  149.9 2.7 %convolution_convert_fusion = bf16[192,2048]{1,0:T(8,128)(2,1)S(1)} fusion(bf16[192,768]{1,0:T(8,128)(2,1)S(1)} %bitcast.60, bf16[768,2048]{1,0:T(8,128)(2,1)} %all-gather.2.cloned.1.call-done), kind=kOutput, calls=%fused_computation | convolution fusion | flops 604372992 | bytes 4227072 | tf_op jit(solution)/shard_map/dot_general | solution.py:752
  152.6 10.4 %all_to_all.16 = bf16[2,96,2048]{2,1,0:T(8,128)(2,1)S(1)} all-to-all(bf16[2,96,2048]{2,1,0:T(8,128)(2,1)S(1)} %bitcast.55), channel_id=1, replica_groups=mesh['sp'=4,'fs'=4,'tp'=2] {'tp'}, dimensions={0} | all-to-all | bytes 1572864 | tf_op jit(solution)/shard_map/all_to_all | solution.py:755
  163.0 1.0 reduce_sum.42
  (52 shorter events, 1.3 us)
Async XLA Ops:
  6.5 135.1 %copy-start = (bf16[512,512]{1,0:T(8,128)(2,1)S(1)}, bf16[512,512]{1,0:T(8,128)(2,1)}, u32[]{:S(2)}) copy-start(bf16[512,512]{1,0:T(8,128)(2,1)} %param.34) | copy-start | bytes 1572868
  6.5 4.2 %copy-start.4 = (bf16[128,512]{1,0:T(8,128)(2,1)S(1)}, bf16[128,512]{1,0:T(8,128)(2,1)}, u32[]{:S(2)}) copy-start(bf16[128,512]{1,0:T(8,128)(2,1)} %param.28) | copy-start | bytes 393220
  6.5 4.5 %copy-start.5 = (bf16[128,512]{1,0:T(8,128)(2,1)S(1)}, bf16[128,512]{1,0:T(8,128)(2,1)}, u32[]{:S(2)}) copy-start(bf16[128,512]{1,0:T(8,128)(2,1)} %param.29) | copy-start | bytes 393220
  6.5 4.8 %copy-start.6 = (bf16[128,512]{1,0:T(8,128)(2,1)S(1)}, bf16[128,512]{1,0:T(8,128)(2,1)}, u32[]{:S(2)}) copy-start(bf16[128,512]{1,0:T(8,128)(2,1)} %param.30) | copy-start | bytes 393220
  6.5 5.0 %copy-start.7 = (bf16[128,256]{1,0:T(8,128)(2,1)S(1)}, bf16[128,256]{1,0:T(8,128)(2,1)}, u32[]{:S(2)}) copy-start(bf16[128,256]{1,0:T(8,128)(2,1)} %param.24) | copy-start | bytes 196612
  6.5 143.4 %all-gather.2.cloned.1.call-start = ((), (), s32[]{:S(2)}) async-start(), calls=%async_computation.3 | async-start | bytes 3342336 | tf_op jit(solution)/shard_map/all_gather | solution.py:695
  8.3 3.6 %copy-start.8 = (bf16[128,256]{1,0:T(8,128)(2,1)S(1)}, bf16[128,256]{1,0:T(8,128)(2,1)}, u32[]{:S(2)}) copy-start(bf16[128,256]{1,0:T(8,128)(2,1)} %param.25) | copy-start | bytes 196612
  9.3 2.8 %copy-start.9 = (bf16[128,256]{1,0:T(8,128)(2,1)S(1)}, bf16[128,256]{1,0:T(8,128)(2,1)}, u32[]{:S(2)}) copy-start(bf16[128,256]{1,0:T(8,128)(2,1)} %param.26) | copy-start | bytes 196612
  9.5 2.9 %copy-start.3 = (bf16[1,192,2048]{2,1,0:T(8,128)(2,1)S(1)}, bf16[1,192,2048]{2,1,0:T(8,128)(2,1)}, u32[]{:S(2)}) copy-start(bf16[1,192,2048]{2,1,0:T(8,128)(2,1)} %param.20) | copy-start | bytes 2359300
  10.9 1.8 %copy-start.13 = (f32[256]{0:T(256)S(1)}, f32[256]{0:T(256)}, u32[]{:S(2)}) copy-start(f32[256]{0:T(256)} %param.33) | copy-start | bytes 3076
  10.9 1.8 %copy-start.10 = (f32[2048]{0:T(1024)S(1)}, f32[2048]{0:T(1024)}, u32[]{:S(2)}) copy-start(f32[2048]{0:T(1024)} %param.23) | copy-start | bytes 24580
  11.7 1.2 copy-start.12
  13.3 97.1 %copy-start.11 = (f32[31,256]{1,0:T(8,128)S(1)}, f32[31,256]{1,0:T(8,128)}, u32[]{:S(2)}) copy-start(f32[31,256]{1,0:T(8,128)} %param.32) | copy-start | bytes 95236
  106.6 1.1 copy-start.1
  110.5 1.3 copy-start.2
  126.1 14.8 %all-to-all-start = ((bf16[8,96,256]{2,1,0:T(8,128)(2,1)}), bf16[8,96,256]{2,1,0:T(8,128)(2,1)S(1)}, u32[]{:S(2)}, u32[]{:S(2)}) async-start(bf16[8,96,256]{2,1,0:T(8,128)(2,1)} %bitcast.24), calls=%async_computation | async-start | bytes 786432 | tf_op jit(solution)/shard_map/all_to_all | solution.py:726
Sparse Core Ops, SparseCore 0:
  9.5 80.9 all-gather.1
